TPU v7x, 512 devices: a whole 4x4x16 slice. The times are simulated.
512 devices in a mesh: sp: 32 (over z, core), tp: 16 (over y, x).
Axes of the slice: x: 4, y: 4, z: 16, core: 2. Of those that a mesh axis runs over, the one named last changes fastest.
Arguments:
- query_pre: bfloat16 [16384, 2048], P('sp', 'tp'), may hold values from -6 to 6
- forget_pre: bfloat16 [16384, 2048], P('sp', 'tp'), may hold values from -8 to 8
- values_in: bfloat16 [16384, 2048], P('sp', 'tp'), may hold values from -16 to 16
- gate_pre: bfloat16 [16384, 2048], P('sp', 'tp'), may hold values from -6 to 6
- floor_gap: float32 [2048], P('tp'), may hold values from 0 to 1, as said below
- head_gain: float32 [128], replicated, may hold values from 0.1 to 1.9
- stream: bfloat16 [16384, 2048], P('sp', 'tp'), may hold values from -40 to 40
- out_proj: bfloat16 [2048, 2048], P(None, 'tp'), may hold values from -0.125 to 0.125
- norm_gain: float32 [2048], P('tp'), may hold values from 0.1 to 1.9
- route_ids: int32 [16384, 2], P('sp'), may hold values from 0 to 31, all different within a row; in each aligned block of 512 rows (0 to 511, 512 to 1023, ...) at most 64 rows name the same one
- route_weights: float32 [16384, 2], P('sp'), may hold values from 0.1 to 1.5
- expert_gate: bfloat16 [32, 2048, 2048], P('sp', None, 'tp'), may hold values from -0.125 to 0.125
- expert_up: bfloat16 [32, 2048, 2048], P('sp', None, 'tp'), may hold values from -0.125 to 0.125
- expert_down: bfloat16 [32, 2048, 2048], P('sp', None, 'tp'), may hold values from -0.125 to 0.125
- shared_gate: bfloat16 [2048, 2048], P(None, 'tp'), may hold values from -0.125 to 0.125
- shared_up: bfloat16 [2048, 2048], P(None, 'tp'), may hold values from -0.125 to 0.125
- shared_down: bfloat16 [2048, 2048], P(None, 'tp'), may hold values from -0.125 to 0.125
Outputs:
- layer_out: bfloat16 [16384, 2048], P('sp', 'tp')
Inputs may be any that keep to these rules, and one draw needn't show every extreme that they name: `route_ids`: in each aligned block of 512 rows every expert is named by at most 64 rows, a bound that some block reaches; the 2 experts of a row differ. `floor_gap`: every entry is positive and at most 0.12.
All inputs are finite; a program needn't handle non-finite values.
Results may differ from a plain program's by a relative error of at most 0.008.
Values may be sent and summed in bfloat16 or wider, within the bound.
A program may use at most 64 MiB of HBM per device.

v0:
```python
import jax
import jax.numpy as jnp
from jax import lax
from jax.sharding import Mesh
from jax.sharding import PartitionSpec as P

D = 2048
HEAD = 128
SPAN = 64
TOP_K = 2
SP = ("sp_0", "sp_1")
TP = ("tp_0", "tp_1")
EPS = 1e-06


def neutral_like(value, identity):
    return jax.tree.map(
        lambda a, e: jnp.broadcast_to(jnp.asarray(e, a.dtype), a.shape), value, identity
    )


def gathered_once(value, axis):
    leaves = jax.tree.leaves(value)
    order = sorted(range(len(leaves)), key=lambda k: -leaves[k].size)
    width = (1, *leaves[order[0]].shape)[-1]
    lines = [
        jnp.pad(leaves[k].reshape(-1), (0, -leaves[k].size % width)).reshape(-1, width)
        for k in order
    ]
    both, at, found = (lax.all_gather(jnp.concatenate(lines), axis), 0, {})
    for k, line in zip(order, lines):
        slab = both[:, at : at + len(line)].reshape(len(both), -1)
        found[k] = slab[:, : leaves[k].size].reshape(-1, *leaves[k].shape)
        at += len(line)
    numbers = iter(range(len(leaves)))
    return jax.tree.map(lambda _: found[next(numbers)], value)


def prefix_by_axis(value, axes, combine, identity):
    before = start = neutral_like(value, identity)
    total = value
    for axis in reversed(axes):
        peers, mine = (lax.axis_size(axis), lax.axis_index(axis))
        pieces = gathered_once(total, axis)
        inside, total = (start, start)
        for k in range(peers):
            passed = k < mine
            total = combine(total, jax.tree.map(lambda part: part[k], pieces))
            inside = jax.tree.map(lambda new, old: jnp.where(passed, new, old), total, inside)
        before = combine(inside, before)
    return before


def sent_to_all(value, axis):
    copies = jnp.broadcast_to(value, (lax.axis_size(axis), *value.shape))
    return lax.all_to_all(copies, axis, split_axis=0, concat_axis=0, tiled=True)


def joined_along(pieces, dim):
    lengths = list(pieces.shape[1:])
    lengths[dim] *= pieces.shape[0]
    return jnp.moveaxis(pieces, 0, dim).reshape(lengths)


def gather_directly(value, axis, dim):
    pieces = sent_to_all(value, axis)
    return joined_along(pieces, dim)


def one_axis_at_a_time(value, axes):
    for axis in axes:
        value = lax.psum(value, axis)
    return value


def sent_together(arrays, axis, dim, along):
    widths = [a.shape[along] for a in arrays]
    both = jnp.concatenate(arrays, axis=along)
    filled = lax.all_gather(both, axis, axis=dim, tiled=True)
    return tuple(jnp.split(filled, [sum(widths[:k]) for k in range(1, len(widths))], axis=along))


def span_step(memory, blocks):
    queries, leakage, values, log_keep = blocks
    length = queries.shape[1]
    growth = jnp.cumsum(log_keep, axis=1)
    causal = jnp.tril(jnp.ones((length, length), dtype=bool))
    spread = growth[:, :, None, :] - growth[:, None, :, :]
    decays = jnp.exp(jnp.where(causal[None, :, :, None], spread, -jnp.inf))
    scores = jnp.einsum("htd,hsd,htsd->hts", queries, leakage, decays)
    within = jnp.einsum("hts,hsv->htv", scores, values)
    carried = jnp.einsum("htd,hdv->htv", queries * jnp.exp(growth), memory)
    closing = growth[:, -1:, :]
    memory = jnp.exp(closing[:, 0, :, None]) * memory + jnp.einsum(
        "hsd,hsv->hdv", leakage * jnp.exp(closing - growth), values
    )
    return (memory, within + carried)


def recurrence(queries, leakage, values, log_keep, memory):
    head_count, length, channels = queries.shape
    number = length // SPAN

    def blocked(array):
        return array.reshape(head_count, number, SPAN, channels).transpose(1, 0, 2, 3)

    memory, outputs = lax.scan(
        span_step, memory, (blocked(queries), blocked(leakage), blocked(values), blocked(log_keep))
    )
    return outputs.transpose(1, 0, 2, 3).reshape(head_count, length, channels)


def chain(earlier, later):
    return (earlier[0] * later[0], later[0][:, :, None] * earlier[1] + later[1])


def pad_rows(array):
    return jnp.concatenate([array, jnp.zeros((1, array.shape[1]), array.dtype)], axis=0)


def matmul(left, right):
    return jnp.dot(left, right, preferred_element_type=jnp.float32)


def body(
    query_pre,
    forget_pre,
    values_in,
    gate_pre,
    floor_gap,
    head_gain,
    stream,
    out_proj,
    norm_gain,
    route_ids,
    route_weights,
    expert_gate,
    expert_up,
    expert_down,
    shared_gate,
    shared_up,
    shared_down,
):
    length, local = query_pre.shape
    head_count = local // HEAD

    def split_heads(array):
        return array.astype(jnp.float32).reshape(length, head_count, HEAD).transpose(1, 0, 2)

    queries = jax.nn.silu(split_heads(query_pre))
    leakage = floor_gap.reshape(head_count, 1, HEAD) * jax.nn.sigmoid(-split_heads(forget_pre))
    log_keep = jnp.log1p(-leakage)
    values = split_heads(values_in)
    growth = jnp.cumsum(log_keep, axis=1)
    closing = growth[:, -1:, :]
    summary = jnp.einsum("hsd,hsv->hdv", leakage * jnp.exp(closing - growth), values)
    through = jnp.exp(closing[:, 0, :])
    unused, incoming = prefix_by_axis(
        (through, summary), SP, chain, (jnp.ones_like(through), jnp.zeros_like(summary))
    )
    outputs = recurrence(queries, leakage, values, log_keep, jnp.zeros_like(summary))
    outputs = outputs + jnp.einsum("htd,hdv->htv", queries * jnp.exp(growth), incoming)
    scaled = (
        outputs * lax.rsqrt(jnp.mean(outputs * outputs, axis=2, keepdims=True) + EPS) * head_gain
    )
    gated = scaled * jax.nn.silu(split_heads(gate_pre))
    mixed = gated.transpose(1, 0, 2).reshape(length, local).astype(jnp.bfloat16)
    projected = matmul(gather_directly(mixed, TP, 1), out_proj)
    residual = stream.astype(jnp.float32) + projected
    squares = one_axis_at_a_time(jnp.sum(residual * residual, axis=1), TP)
    normed = (residual * lax.rsqrt(squares / D + EPS)[:, None] * norm_gain).astype(jnp.bfloat16)
    experts = lax.axis_size(SP) * expert_gate.shape[0]
    capacity = 2 * TOP_K * length // experts
    flat_ids = route_ids.reshape(-1)
    matches = (flat_ids[:, None] == jnp.arange(experts, dtype=jnp.int32)[None, :]).astype(jnp.int32)
    earlier_hits = jnp.cumsum(matches, axis=0) - matches
    target = flat_ids * capacity + jnp.sum(earlier_hits * matches, axis=1)
    sender = (
        jnp.full((experts * capacity,), length, jnp.int32)
        .at[target]
        .set(jnp.arange(length * TOP_K, dtype=jnp.int32) // TOP_K)
    )
    gate_slice = expert_gate[0]
    up_slice = expert_up[0]
    down_slice = expert_down[0]
    arrived = lax.all_to_all(pad_rows(normed)[sender], SP, split_axis=0, concat_axis=0, tiled=True)
    own_rows, routed_rows = sent_together((normed, arrived), TP, 1, 0)
    shared_gate_part = matmul(own_rows, shared_gate)
    shared_up_part = matmul(own_rows, shared_up)
    routed_gate_part = matmul(routed_rows, gate_slice)
    routed_up_part = matmul(routed_rows, up_slice)
    shared_hidden = (jax.nn.silu(shared_gate_part) * shared_up_part).astype(jnp.bfloat16)
    routed_hidden = (jax.nn.silu(routed_gate_part) * routed_up_part).astype(jnp.bfloat16)
    full_shared, full_routed = (
        lax.all_gather(shared_hidden, TP, axis=1, tiled=True),
        lax.all_gather(routed_hidden, TP, axis=1, tiled=True),
    )
    shared_out = matmul(full_shared, shared_down)
    expert_result = matmul(full_routed, down_slice).astype(jnp.bfloat16)
    returned = lax.all_to_all(expert_result, SP, split_axis=0, concat_axis=0, tiled=True)
    picked = returned[target].astype(jnp.float32).reshape(length, TOP_K, returned.shape[1])
    routed = jnp.sum(picked * route_weights[:, :, None], axis=1)
    return (residual + shared_out + routed).astype(jnp.bfloat16)


def solution(mesh):
    finer = Mesh(mesh.devices.reshape(16, 2, 4, 4), ("sp_0", "sp_1", "tp_0", "tp_1"))
    in_specs = (
        P(SP, TP),
        P(SP, TP),
        P(SP, TP),
        P(SP, TP),
        P(TP),
        P(),
        P(SP, TP),
        P(None, TP),
        P(TP),
        P(SP, None),
        P(SP, None),
        P(SP, None, TP),
        P(SP, None, TP),
        P(SP, None, TP),
        P(None, TP),
        P(None, TP),
        P(None, TP),
    )
    out_specs = P(SP, TP)
    return jax.shard_map(body, mesh=finer, in_specs=in_specs, out_specs=out_specs, check_vma=False)
```

profile of v0, /device:TPU:2, one launch (start us, length us, event | category | flops | bytes accessed | tf_op | source)
XLA Modules:
  0.0 454.3 jit_solution(16247520927167944288)
XLA Ops:
  13.5 24.4 %while.13 = (s32[]{:T(128)}, f32[1,128,128]{2,1,0:T(8,128)S(1)}, f32[8,1,64,128]{3,2,1,0:T(8,128)S(1)}, f32[8,1,64,128]{3,2,1,0:T(8,128)S(1)}, f32[8,1,64,128]{3...) while((s32[]{:T(128)}, f32[1,128,128]{2,1,0:T(8,128)S(1)}, ...), condition=%wide.region_2.3_spmd.clone, body=%wide.region_0.0_spmd.clone.sunk | while | flops 8478723 | bytes 5051520 | solution.py:107
  38.2 50.0 %all-gather.15.cloned.1.call-done = f32[16,129,128]{2,1,0:T(8,128)} async-done(((f32[1,129,128]{2,1,0:T(8,128)}), f32[16,129,128]{2,1,0:T(8,128)}) %all-gather.15.cloned.1.call-update) | async-done | bytes 1056784 | tf_op jit(solution)/shard_map/all_gather | solution.py:30
  89.0 1.9 multiply_reduce_fusion.1
  92.6 7.4 %all-to-all-start = ((bf16[16,512,128]{1,2,0:T(8,128)(2,1)}), bf16[16,512,128]{1,2,0:T(8,128)(2,1)S(1)}, u32[]{:S(2)}, u32[]{:S(2)}) async-start(bf16[16,512,128]{1,2,0:T(8,128)(2,1)} %broadcast_in_dim.48), calls=%async_computation | async-start | bytes 4194304 | tf_op jit(solution)/shard_map/all_to_all | solution.py:56
  100.6 9.0 %reduce-window.16 = s32[32,8,128]{2,1,0:T(8,128)S(1)} reduce-window(s32[32,8,128]{2,1,0:T(8,128)S(1)} %fusion.72, s32[]{:T(128)} %constant.41.clone.1), window={size=1x1x128 pad=0_0x0_0x127_0}, to_apply=%region_9.10 | reduce-window | flops 4161536 | bytes 262148 | tf_op jit(solution)/shard_map/reduce-window.2
  110.5 4.3 scatter_custom_fusion
  114.8 3.6 all-to-all-done
  120.3 11.1 %psum.14 = f32[512]{0:T(512)S(1)} all-reduce(f32[512]{0:T(512)S(1)} %get-tuple-element.138), channel_id=1, replica_groups=mesh['sp_0'=16,'sp_1'=2,'tp_0'=4,'tp_1'=4] {'tp_0'}, use_global_device_ids=true, to_apply=%region_7.8 | all-reduce | flops 512 | bytes 4096 | tf_op jit(solution)/shard_map/psum | solution.py:72
  131.4 9.5 %psum.15 = f32[512]{0:T(512)S(1)} all-reduce(f32[512]{0:T(512)S(1)} %psum.14), channel_id=1, replica_groups=mesh['sp_0'=16,'sp_1'=2,'tp_0'=4,'tp_1'=4] {'tp_1'}, use_global_device_ids=true, to_apply=%region_8.9 | all-reduce | flops 512 | bytes 4096 | tf_op jit(solution)/shard_map/psum | solution.py:72
  141.1 6.2 %gather_fusion = bf16[2048,128]{1,0:T(8,128)(2,1)S(1)} fusion(bf16[513,128]{1,0:T(8,128)(2,1)S(1)} %concatenate.14, s32[2048]{0:T(1024)S(1)} %fusion.147), kind=kCustom, calls=%fused_computation | custom fusion | bytes 1056768 | tf_op jit(solution)/shard_map/gather | solution.py:186
  147.3 41.7 %all_to_all.29 = bf16[32,64,128]{2,1,0:T(8,128)(2,1)S(1)} all-to-all(bf16[32,64,128]{2,1,0:T(8,128)(2,1)S(1)} %bitcast.243), channel_id=1, replica_groups=mesh['sp_0'=16,'sp_1'=2,'tp_0'=4,'tp_1'=4] {'sp_0','sp_1'}, dimensions={0} | all-to-all | bytes 1048576 | tf_op jit(solution)/shard_map/all_to_all | solution.py:186
  190.1 90.3 %all-gather.9.cloned.1.call-done = bf16[2560,2048]{1,0:T(8,128)(2,1)} async-done(((bf16[2560,128]{1,0:T(8,128)(2,1)}), bf16[2560,2048]{1,0:T(8,128)(2,1)}) %all-gather.9.cloned.1.call-update) | async-done | bytes 10485776 | tf_op jit(solution)/shard_map/all_gather | solution.py:79
  280.4 5.9 %fusion.30 = f32[2048,128]{1,0:T(8,128)S(1)} fusion(bf16[2560,2048]{1,0:T(8,128)(2,1)} %all-gather.9.cloned.1.call-done, bf16[1,2048,128]{2,1,0:T(8,128)(2,1)S(1)} %copy-done), kind=kOutput, calls=%fused_computation.42 | convolution fusion | flops 1073741824 | bytes 9961472 | tf_op jit(solution)/shard_map/dot_general | solution.py:122
  286.8 3.2 fusion.35
  290.1 2.5 fusion.40
  292.6 3.1 fusion.47
  295.8 86.4 %all-gather.13.cloned.1.call-done = bf16[2048,2048]{1,0:T(8,128)(2,1)} async-done(((bf16[2048,128]{1,0:T(8,128)(2,1)}), bf16[2048,2048]{1,0:T(8,128)(2,1)}) %all-gather.13.cloned.1.call-update) | async-done | bytes 8388624 | tf_op jit(solution)/shard_map/all_gather | solution.py:196
  382.2 6.5 %convolution_convert_fusion = bf16[2048,128]{1,0:T(8,128)(2,1)} fusion(bf16[2048,2048]{1,0:T(8,128)(2,1)} %all-gather.13.cloned.1.call-done, bf16[1,2048,128]{2,1,0:T(8,128)(2,1)S(1)} %copy-done.15), kind=kOutput, calls=%fused_computation.45 | convolution fusion | flops 1074003968 | bytes 9437184 | tf_op jit(solution)/shard_map/dot_general | solution.py:122
  388.7 12.7 %all-to-all-start.2 = ((bf16[32,64,128]{2,1,0:T(8,128)(2,1)}), bf16[32,64,128]{2,1,0:T(8,128)(2,1)S(1)}, u32[]{:S(2)}, u32[]{:S(2)}) async-start(bf16[32,64,128]{2,1,0:T(8,128)(2,1)} %bitcast.52), calls=%async_computation.2 | async-start | bytes 1048576 | tf_op jit(solution)/shard_map/all_to_all | solution.py:200
  401.6 33.6 %all-to-all-done.2 = bf16[32,64,128]{2,1,0:T(8,128)(2,1)S(1)} async-done(((bf16[32,64,128]{2,1,0:T(8,128)(2,1)}), bf16[32,64,128]{2,1,0:T(8,128)(2,1)S(1)}, u32[]{:S(2)}, u32[]{:S(2)}) %all-to-all-start.2) | async-done | bytes 524320 | tf_op jit(solution)/shard_map/all_to_all | solution.py:200
  435.2 3.2 gather_fusion.1
  438.4 2.8 fusion.50
  441.2 3.5 all-gather.11.cloned.1.call-done
  444.8 3.0 fusion.46
  (187 shorter events, 38.6 us)
Async XLA Ops:
  6.5 273.9 %copy-start = (bf16[1,2048,128]{2,1,0:T(8,128)(2,1)S(1)}, bf16[1,2048,128]{2,1,0:T(8,128)(2,1)}, u32[]{:S(2)}) copy-start(bf16[1,2048,128]{2,1,0:T(8,128)(2,1)} %param.30) | copy-start | bytes 1572868
  6.5 81.7 %all-gather.15.cloned.1.call-start = ((), (), s32[]{:S(2)}) async-start(), calls=%async_computation.6 | async-start | bytes 1183744 | tf_op jit(solution)/shard_map/all_gather | solution.py:30
  8.4 1.4 copy-start.2
  8.5 1.4 copy-start.8
  9.6 3.5 copy-start.4
  13.5 24.6 %copy-start.5 = (bf16[512,128]{1,0:T(8,128)(2,1)S(1)}, bf16[512,128]{1,0:T(8,128)(2,1)}, u32[]{:S(2)}) copy-start(bf16[512,128]{1,0:T(8,128)(2,1)} %param.22) | copy-start | bytes 393220
  37.9 53.0 %copy-start.9 = (f32[128]{0:T(128)S(1)}, f32[128]{0:T(128)}, u32[]{:S(2)}) copy-start(f32[128]{0:T(128)} %param.24) | copy-start | bytes 1540
  92.6 7.5 %copy-start.6 = (s32[512,2]{0,1:T(2,128)S(1)}, s32[512,2]{0,1:T(2,128)}, u32[]{:S(2)}) copy-start(s32[512,2]{0,1:T(2,128)} %param.28) | copy-start | bytes 12292
  92.6 25.8 %all-to-all-start = ((bf16[16,512,128]{1,2,0:T(8,128)(2,1)}), bf16[16,512,128]{1,2,0:T(8,128)(2,1)S(1)}, u32[]{:S(2)}, u32[]{:S(2)}) async-start(bf16[16,512,128]{1,2,0:T(8,128)(2,1)} %broadcast_in_dim.48), calls=%async_computation | async-start | bytes 4194304 | tf_op jit(solution)/shard_map/all_to_all | solution.py:56
  100.0 18.4 %copy-start.3 = (bf16[512,128]{1,0:T(8,128)(2,1)S(1)}, bf16[512,128]{1,0:T(8,128)(2,1)}, u32[]{:S(2)}) copy-start(bf16[512,128]{1,0:T(8,128)(2,1)} %param.25) | copy-start | bytes 393220
  100.0 180.4 %all-gather.9.cloned.1.call-start = ((), (), s32[]{:S(2)}) async-start(), calls=%async_computation.3 | async-start | bytes 11141120 | tf_op jit(solution)/shard_map/all_gather | solution.py:79
  109.7 31.2 %copy-start.10 = (f32[128]{0:T(128)S(1)}, f32[128]{0:T(128)}, u32[]{:S(2)}) copy-start(f32[128]{0:T(128)} %param.27) | copy-start | bytes 1540
  189.9 96.5 %copy-start.12 = (bf16[1,2048,128]{2,1,0:T(8,128)(2,1)S(1)}, bf16[1,2048,128]{2,1,0:T(8,128)(2,1)}, u32[]{:S(2)}) copy-start(bf16[1,2048,128]{2,1,0:T(8,128)(2,1)} %param.31) | copy-start | bytes 1572868
  189.9 192.3 %all-gather.13.cloned.1.call-start = ((), (), s32[]{:S(2)}) async-start(), calls=%async_computation.5 | async-start | bytes 8912896 | tf_op jit(solution)/shard_map/all_gather | solution.py:196
  280.4 6.4 %copy-start.11 = (bf16[2560,2048]{1,0:T(8,128)(2,1)S(1)}, bf16[2560,2048]{1,0:T(8,128)(2,1)}, u32[]{:S(2)}) copy-start(bf16[2560,2048]{1,0:T(8,128)(2,1)} %all-gather.9.cloned.1.call-done) | copy-start | bytes 31457284
  286.8 3.3 copy-start.13
  290.0 2.6 copy-start.14
  290.1 154.7 %all-gather.11.cloned.1.call-start = ((), (), s32[]{:S(2)}) async-start(), calls=%async_computation.4 | async-start | bytes 2228224 | tf_op jit(solution)/shard_map/all_gather | solution.py:195
  292.6 89.6 %copy-start.15 = (bf16[1,2048,128]{2,1,0:T(8,128)(2,1)S(1)}, bf16[1,2048,128]{2,1,0:T(8,128)(2,1)}, u32[]{:S(2)}) copy-start(bf16[1,2048,128]{2,1,0:T(8,128)(2,1)} %param.32) | copy-start | bytes 1572868
  295.8 105.7 %copy-start.7 = (f32[512,2]{0,1:T(2,128)S(1)}, f32[512,2]{0,1:T(2,128)}, u32[]{:S(2)}) copy-start(f32[512,2]{0,1:T(2,128)} %param.29) | copy-start | bytes 12292
  388.7 56.0 %copy-start.1 = (bf16[2048,128]{1,0:T(8,128)(2,1)S(1)}, bf16[2048,128]{1,0:T(8,128)(2,1)}, u32[]{:S(2)}) copy-start(bf16[2048,128]{1,0:T(8,128)(2,1)} %param.35) | copy-start | bytes 1572868
  388.7 46.5 %all-to-all-start.2 = ((bf16[32,64,128]{2,1,0:T(8,128)(2,1)}), bf16[32,64,128]{2,1,0:T(8,128)(2,1)S(1)}, u32[]{:S(2)}, u32[]{:S(2)}) async-start(bf16[32,64,128]{2,1,0:T(8,128)(2,1)} %bitcast.52), calls=%async_computation.2 | async-start | bytes 1048576 | tf_op jit(solution)/shard_map/all_to_all | solution.py:200
Sparse Core Ops, SparseCore 0:
  13.0 75.1 all-gather.14
  190.0 90.3 all-gather.8
  290.2 91.9 all-gather.12
  385.1 59.6 all-gather.10
where the time goes:
time: 455 us; the launch traced here: 454 us
  waiting for transfers between devices  268 us (59%)
  blocking collectives  64.2 us (14%)
  other arithmetic  35.4 us (8%)
  matrix products  32.5 us (7%)
  starting transfers between devices  20.4 us (4%)
  local copies, waits for them, and re-layouts  20.2 us (4%)
  between operations  13.7 us (3%)
    all_gather x1, waiting for transfers between devices, sent_together(): filled = lax.all_gather(both, axis, axis=dim, tiled=True)  90.3 us
    all_gather x1, waiting for transfers between devices, body(): lax.all_gather(routed_hidden, TP, axis=1, tiled=True)  86.4 us
    all_gather x1, waiting for transfers between devices, gathered_once(): both, at, found = (lax.all_gather(jnp.concatenate(lines), axis), 0, {})  50 us
    all_to_all x1, blocking collectives, body(): lax.all_to_all(pad_rows(normed)[sender], SP, split_axis=0, concat_axis=0,...  41.7 us
    all_to_all x1, waiting for transfers between devices, body(): lax.all_to_all(expert_result, SP, split_axis=0, concat_axis=0, tiled=True)  33.6 us
    dot_general x7, matrix products, matmul(): return jnp.dot(left, right, preferred_element_type=jnp.float32)  26.2 us
    psum x2, blocking collectives, one_axis_at_a_time(): value = lax.psum(value, axis)  20.6 us
    dot_general x8, other arithmetic, span_step(): scores = jnp.einsum('htd,hsd,htsd->hts', queries, leakage, decays)  13.8 us
  transfers between devices with their start and end apart: 6, of which 6 were waited for; matrix products, arithmetic and copies ran while one was open for 13% of the time, Pallas kernels for 0%

commit v1 on v0

--- a/solution.py
+++ b/solution.py
@@ -191,9 +191,15 @@
     routed_up_part = matmul(routed_rows, up_slice)
     shared_hidden = (jax.nn.silu(shared_gate_part) * shared_up_part).astype(jnp.bfloat16)
     routed_hidden = (jax.nn.silu(routed_gate_part) * routed_up_part).astype(jnp.bfloat16)
+    place_arrays = lambda local_array: jnp.concatenate(
+        lax.all_to_all(
+            jnp.stack(lax.axis_size(TP) * [local_array]), axis_name=TP, split_axis=0, concat_axis=0
+        ),
+        axis=1,
+    )
     full_shared, full_routed = (
         lax.all_gather(shared_hidden, TP, axis=1, tiled=True),
-        lax.all_gather(routed_hidden, TP, axis=1, tiled=True),
+        place_arrays(routed_hidden),
     )
     shared_out = matmul(full_shared, shared_down)
     expert_result = matmul(full_routed, down_slice).astype(jnp.bfloat16)

time: 455 us -> 501 us (1.10)
  the two profiles are of different devices: /device:TPU:2 before, /device:TPU:1 now
where the time goes in v1:
time: 501 us
  waiting for transfers between devices  283 us (56%)
  blocking collectives  77.6 us (15%)
  other arithmetic  38 us (8%)
  starting transfers between devices  30.8 us (6%)
  matrix products  30.6 us (6%)
  local copies, waits for them, and re-layouts  26.3 us (5%)
  between operations  13.7 us (3%)
    all_to_all x1, waiting for transfers between devices, body(): lax.all_to_all(jnp.stack(lax.axis_size(TP) * [local_array]), axis_name=TP...  122 us
    all_gather x1, waiting for transfers between devices, sent_together(): filled = lax.all_gather(both, axis, axis=dim, tiled=True)  89.2 us
    all_to_all x1, blocking collectives, body(): lax.all_to_all(pad_rows(normed)[sender], SP, split_axis=0, concat_axis=0,...  54.8 us
    all_gather x1, waiting for transfers between devices, gathered_once(): both, at, found = (lax.all_gather(jnp.concatenate(lines), axis), 0, {})  33.6 us
    all_to_all x1, waiting for transfers between devices, body(): lax.all_to_all(expert_result, SP, split_axis=0, concat_axis=0, tiled=True)  33.3 us
    dot_general x7, matrix products, matmul(): return jnp.dot(left, right, preferred_element_type=jnp.float32)  24.3 us
    all_to_all x1, starting transfers between devices, body(): lax.all_to_all(expert_result, SP, split_axis=0, concat_axis=0, tiled=True)  18.8 us
    psum x2, blocking collectives, one_axis_at_a_time(): value = lax.psum(value, axis)  14.4 us
  transfers between devices with their start and end apart: 6, of which 5 were waited for; matrix products, arithmetic and copies ran while one was open for 12% of the time, Pallas kernels for 0%

profile of v1, /device:TPU:1, one launch (start us, length us, event | category | flops | bytes accessed | tf_op | source)
XLA Modules:
  0.0 500.7 jit_solution(8711588817396343911)
XLA Ops:
  10.2 8.4 %all-gather.2 = f32[2,129,128]{2,1,0:T(8,128)S(1)} all-gather(f32[1,129,128]{2,1,0:T(8,128)S(1)} %maximum_bitcast_fusion), channel_id=2, replica_groups=mesh['sp_0'=16,'sp_1'=2,'tp_0'=4,'tp_1'=4] {'sp_1'}, dimensions={0}, use_global_device_ids=true | all-gather | bytes 198144 | tf_op jit(solution)/shard_map/all_gather | solution.py:30
  20.0 24.4 %while.13 = (s32[]{:T(128)}, f32[1,128,128]{2,1,0:T(8,128)S(1)}, f32[8,1,64,128]{3,2,1,0:T(8,128)S(1)}, f32[8,1,64,128]{3,2,1,0:T(8,128)S(1)}, f32[8,1,64,128]{3...) while((s32[]{:T(128)}, f32[1,128,128]{2,1,0:T(8,128)S(1)}, ...), condition=%wide.region_2.3_spmd.clone, body=%wide.region_0.0_spmd.clone.sunk | while | flops 8478723 | bytes 5052550 | solution.py:107
  44.8 33.6 %all-gather.12.cloned.1.call-done = f32[16,129,128]{2,1,0:T(8,128)} async-done(((f32[1,129,128]{2,1,0:T(8,128)}), f32[16,129,128]{2,1,0:T(8,128)}) %all-gather.12.cloned.1.call-update) | async-done | bytes 1056784 | tf_op jit(solution)/shard_map/all_gather | solution.py:30
  82.8 7.1 %all-to-all-start = ((bf16[16,512,128]{1,2,0:T(8,128)(2,1)}), bf16[16,512,128]{1,2,0:T(8,128)(2,1)S(1)}, u32[]{:S(2)}, u32[]{:S(2)}) async-start(bf16[16,512,128]{1,2,0:T(8,128)(2,1)} %broadcast_in_dim.48), calls=%async_computation | async-start | bytes 4194304 | tf_op jit(solution)/shard_map/all_to_all | solution.py:56
  92.0 9.0 %reduce-window.16 = s32[32,8,128]{2,1,0:T(8,128)S(1)} reduce-window(s32[32,8,128]{2,1,0:T(8,128)S(1)} %fusion.72, s32[]{:T(128)} %constant.41.clone.1), window={size=1x1x128 pad=0_0x0_0x127_0}, to_apply=%region_9.10 | reduce-window | flops 4161536 | bytes 262148 | tf_op jit(solution)/shard_map/reduce-window.2
  103.5 4.5 scatter_custom_fusion
  108.0 4.6 all-to-all-done
  113.4 7.5 %psum.14 = f32[512]{0:T(512)S(1)} all-reduce(f32[512]{0:T(512)S(1)} %get-tuple-element.138), channel_id=1, replica_groups=mesh['sp_0'=16,'sp_1'=2,'tp_0'=4,'tp_1'=4] {'tp_0'}, use_global_device_ids=true, to_apply=%region_7.8 | all-reduce | flops 512 | bytes 4096 | tf_op jit(solution)/shard_map/psum | solution.py:72
  120.9 6.9 %psum.15 = f32[512]{0:T(512)S(1)} all-reduce(f32[512]{0:T(512)S(1)} %psum.14), channel_id=1, replica_groups=mesh['sp_0'=16,'sp_1'=2,'tp_0'=4,'tp_1'=4] {'tp_1'}, use_global_device_ids=true, to_apply=%region_8.9 | all-reduce | flops 512 | bytes 4096 | tf_op jit(solution)/shard_map/psum | solution.py:72
  128.7 6.2 %gather_fusion = bf16[2048,128]{1,0:T(8,128)(2,1)S(1)} fusion(bf16[513,128]{1,0:T(8,128)(2,1)S(1)} %concatenate.14, s32[2048]{0:T(1024)S(1)} %fusion.147), kind=kCustom, calls=%fused_computation | custom fusion | bytes 1056768 | tf_op jit(solution)/shard_map/gather | solution.py:186
  134.9 54.8 %all_to_all.34 = bf16[32,64,128]{2,1,0:T(8,128)(2,1)S(1)} all-to-all(bf16[32,64,128]{2,1,0:T(8,128)(2,1)S(1)} %bitcast.247), channel_id=1, replica_groups=mesh['sp_0'=16,'sp_1'=2,'tp_0'=4,'tp_1'=4] {'sp_0','sp_1'}, dimensions={0} | all-to-all | bytes 1048576 | tf_op jit(solution)/shard_map/all_to_all | solution.py:186
  190.6 89.2 %all-gather.8.cloned.1.call-done = bf16[2560,2048]{1,0:T(8,128)(2,1)} async-done(((bf16[2560,128]{1,0:T(8,128)(2,1)}), bf16[2560,2048]{1,0:T(8,128)(2,1)}) %all-gather.8.cloned.1.call-update) | async-done | bytes 10485776 | tf_op jit(solution)/shard_map/all_gather | solution.py:79
  279.8 5.9 %fusion.30 = f32[2048,128]{1,0:T(8,128)S(1)} fusion(bf16[2560,2048]{1,0:T(8,128)(2,1)} %all-gather.8.cloned.1.call-done, bf16[1,2048,128]{2,1,0:T(8,128)(2,1)S(1)} %copy-done), kind=kOutput, calls=%fused_computation.42 | convolution fusion | flops 1073741824 | bytes 9961472 | tf_op jit(solution)/shard_map/dot_general | solution.py:122
  288.8 4.5 stack.2
  293.2 4.9 all-to-all-start.2
  298.2 2.5 fusion.40
  300.7 3.1 fusion.47
  303.9 122.3 %all-to-all-done.2 = bf16[16,2048,128]{1,2,0:T(8,128)(2,1)} async-done(((bf16[16,2048,128]{1,2,0:T(8,128)(2,1)}), bf16[16,2048,128]{1,2,0:T(8,128)(2,1)}, u32[]{:S(2)}, u32[]{:S(2)}) %all-to-all-start.2) | async-done | bytes 8388640 | tf_op jit(solution)/shard_map/all_to_all | solution.py:195
  426.2 6.6 %convolution_convert_fusion = bf16[2048,128]{1,0:T(8,128)(2,1)} fusion(bf16[2048,2048]{0,1:T(8,128)(2,1)} %bitcast.52, bf16[1,2048,128]{2,1,0:T(8,128)(2,1)S(1)} %copy-done.15), kind=kOutput, calls=%fused_computation.45 | convolution fusion | flops 1074003968 | bytes 9437184 | tf_op jit(solution)/shard_map/dot_general | solution.py:122
  432.8 18.8 %all-to-all-start.3 = ((bf16[32,64,128]{2,1,0:T(8,128)(2,1)}), bf16[32,64,128]{2,1,0:T(8,128)(2,1)S(1)}, u32[]{:S(2)}, u32[]{:S(2)}) async-start(bf16[32,64,128]{2,1,0:T(8,128)(2,1)} %bitcast.54), calls=%async_computation.3 | async-start | bytes 1048576 | tf_op jit(solution)/shard_map/all_to_all | solution.py:206
  451.7 33.3 %all-to-all-done.3 = bf16[32,64,128]{2,1,0:T(8,128)(2,1)S(1)} async-done(((bf16[32,64,128]{2,1,0:T(8,128)(2,1)}), bf16[32,64,128]{2,1,0:T(8,128)(2,1)S(1)}, u32[]{:S(2)}, u32[]{:S(2)}) %all-to-all-start.3) | async-done | bytes 524320 | tf_op jit(solution)/shard_map/all_to_all | solution.py:206
  485.1 3.2 gather_fusion.1
  488.3 2.8 fusion.50
  491.1 3.0 fusion.46
  (188 shorter events, 43.9 us)
Async XLA Ops:
  6.5 273.2 %copy-start = (bf16[1,2048,128]{2,1,0:T(8,128)(2,1)S(1)}, bf16[1,2048,128]{2,1,0:T(8,128)(2,1)}, u32[]{:S(2)}) copy-start(bf16[1,2048,128]{2,1,0:T(8,128)(2,1)} %param.30) | copy-start | bytes 1572868
  6.5 71.8 %all-gather.12.cloned.1.call-start = ((), (), s32[]{:S(2)}) async-start(), calls=%async_computation.6 | async-start | bytes 1183744 | tf_op jit(solution)/shard_map/all_gather | solution.py:30
  8.4 1.4 copy-start.3
  8.5 1.4 copy-start.9
  9.2 10.2 %copy-start.5 = (bf16[512,128]{1,0:T(8,128)(2,1)S(1)}, bf16[512,128]{1,0:T(8,128)(2,1)}, u32[]{:S(2)}) copy-start(bf16[512,128]{1,0:T(8,128)(2,1)} %param.19) | copy-start | bytes 393220
  20.0 24.5 %copy-start.6 = (bf16[512,128]{1,0:T(8,128)(2,1)S(1)}, bf16[512,128]{1,0:T(8,128)(2,1)}, u32[]{:S(2)}) copy-start(bf16[512,128]{1,0:T(8,128)(2,1)} %param.22) | copy-start | bytes 393220
  44.4 36.6 %copy-start.10 = (f32[128]{0:T(128)S(1)}, f32[128]{0:T(128)}, u32[]{:S(2)}) copy-start(f32[128]{0:T(128)} %param.24) | copy-start | bytes 1540
  82.8 7.2 %copy-start.7 = (s32[512,2]{0,1:T(2,128)S(1)}, s32[512,2]{0,1:T(2,128)}, u32[]{:S(2)}) copy-start(s32[512,2]{0,1:T(2,128)} %param.28) | copy-start | bytes 12292
  82.8 29.8 %all-to-all-start = ((bf16[16,512,128]{1,2,0:T(8,128)(2,1)}), bf16[16,512,128]{1,2,0:T(8,128)(2,1)S(1)}, u32[]{:S(2)}, u32[]{:S(2)}) async-start(bf16[16,512,128]{1,2,0:T(8,128)(2,1)} %broadcast_in_dim.48), calls=%async_computation | async-start | bytes 4194304 | tf_op jit(solution)/shard_map/all_to_all | solution.py:56
  89.9 22.7 %copy-start.1 = (bf16[2048,128]{1,0:T(8,128)(2,1)S(1)}, bf16[2048,128]{1,0:T(8,128)(2,1)}, u32[]{:S(2)}) copy-start(bf16[2048,128]{1,0:T(8,128)(2,1)} %param.26) | copy-start | bytes 1572868
  89.9 22.7 %copy-start.4 = (bf16[512,128]{1,0:T(8,128)(2,1)S(1)}, bf16[512,128]{1,0:T(8,128)(2,1)}, u32[]{:S(2)}) copy-start(bf16[512,128]{1,0:T(8,128)(2,1)} %param.25) | copy-start | bytes 393220
  89.9 189.9 %all-gather.8.cloned.1.call-start = ((), (), s32[]{:S(2)}) async-start(), calls=%async_computation.4 | async-start | bytes 11141120 | tf_op jit(solution)/shard_map/all_gather | solution.py:79
  190.6 95.1 %copy-start.12 = (bf16[1,2048,128]{2,1,0:T(8,128)(2,1)S(1)}, bf16[1,2048,128]{2,1,0:T(8,128)(2,1)}, u32[]{:S(2)}) copy-start(bf16[1,2048,128]{2,1,0:T(8,128)(2,1)} %param.31) | copy-start | bytes 1572868
  279.8 6.4 %copy-start.11 = (bf16[2560,2048]{1,0:T(8,128)(2,1)S(1)}, bf16[2560,2048]{1,0:T(8,128)(2,1)}, u32[]{:S(2)}) copy-start(bf16[2560,2048]{1,0:T(8,128)(2,1)} %all-gather.8.cloned.1.call-done) | copy-start | bytes 31457284
  293.2 5.0 copy-start.13
  293.2 133.0 %all-to-all-start.2 = ((bf16[16,2048,128]{1,2,0:T(8,128)(2,1)}), bf16[16,2048,128]{1,2,0:T(8,128)(2,1)}, u32[]{:S(2)}, u32[]{:S(2)}) async-start(bf16[16,2048,128]{1,2,0:T(8,128)(2,1)} %stack.2), calls=%async_computation.2 | async-start | bytes 16777216 | tf_op jit(solution)/shard_map/all_to_all | solution.py:195
  298.2 2.5 copy-start.14
  298.2 192.9 %all-gather.10.cloned.1.call-start = ((), (), s32[]{:S(2)}) async-start(), calls=%async_computation.5 | async-start | bytes 2228224 | tf_op jit(solution)/shard_map/all_gather | solution.py:201
  300.7 125.5 %copy-start.15 = (bf16[1,2048,128]{2,1,0:T(8,128)(2,1)S(1)}, bf16[1,2048,128]{2,1,0:T(8,128)(2,1)}, u32[]{:S(2)}) copy-start(bf16[1,2048,128]{2,1,0:T(8,128)(2,1)} %param.32) | copy-start | bytes 1572868
  426.2 25.4 %copy-start.8 = (f32[512,2]{0,1:T(2,128)S(1)}, f32[512,2]{0,1:T(2,128)}, u32[]{:S(2)}) copy-start(f32[512,2]{0,1:T(2,128)} %param.29) | copy-start | bytes 12292
  432.8 58.3 %copy-start.2 = (bf16[2048,128]{1,0:T(8,128)(2,1)S(1)}, bf16[2048,128]{1,0:T(8,128)(2,1)}, u32[]{:S(2)}) copy-start(bf16[2048,128]{1,0:T(8,128)(2,1)} %param.35) | copy-start | bytes 1572868
  432.8 52.3 %all-to-all-start.3 = ((bf16[32,64,128]{2,1,0:T(8,128)(2,1)}), bf16[32,64,128]{2,1,0:T(8,128)(2,1)S(1)}, u32[]{:S(2)}, u32[]{:S(2)}) async-start(bf16[32,64,128]{2,1,0:T(8,128)(2,1)} %bitcast.54), calls=%async_computation.3 | async-start | bytes 1048576 | tf_op jit(solution)/shard_map/all_to_all | solution.py:206
Sparse Core Ops, SparseCore 0:
  19.5 58.8 all-gather.11
  190.7 89.0 all-gather.7
  304.0 125.4 all-gather.9
